TPU v7x, 32 devices: a whole 2x2x4 slice. The times are simulated.
32 devices in a mesh: sp: 16 (over z, y, x), tp: 2 (over core).
Axes of the slice: x: 2, y: 2, z: 4, core: 2. Of those that a mesh axis runs over, the one named last changes fastest.
Arguments:
- conv_in: bfloat16 [4096, 1024], P('sp', 'tp'), may hold values from -6 to 6
- gate_outer: bfloat16 [4096, 1024], P('sp', 'tp'), may hold values from -6 to 6
- gate_inner: bfloat16 [4096, 1024], P('sp', 'tp'), may hold values from -6 to 6
- tap_weights: float32 [3, 1024], P(None, 'tp'), may hold values from -3 to 3
- doc_ids: int32 [4096], P('sp'), may hold values from 0 to 7, never falling along the last dimension, each value on 1 to 1024 neighbouring positions
- w_proj: bfloat16 [1024, 2048], replicated, may hold values from -0.1875 to 0.1875
- stream: bfloat16 [4096, 2048], P(('sp', 'tp')), may hold values from -6 to 6
- norm_gain: float32 [2048], replicated, may hold values from 0.1 to 1.9
- routes: int32 [4096, 4], P(('sp', 'tp')), may hold values from 0 to 31, all different within a row; in each aligned block of 128 rows (0 to 127, 128 to 255, ...) at most 32 rows name the same one
- route_weights: float32 [4096, 4], P(('sp', 'tp')), may hold values from 0.1 to 1
- w_gate: bfloat16 [32, 2048, 768], P(('sp', 'tp')), may hold values from -0.5 to 0.5
- w_up: bfloat16 [32, 2048, 768], P(('sp', 'tp')), may hold values from -0.5 to 0.5
- w_down: bfloat16 [32, 768, 2048], P(('sp', 'tp')), may hold values from -0.0546875 to 0.0546875
Outputs:
- layer_out: bfloat16 [4096, 2048], P(('sp', 'tp'))
Inputs may be any that keep to these rules, and one draw needn't show every extreme that they name: `doc_ids`: document numbers never fall along the sequence; a document covers at most 1024 positions. `routes`: a token names 4 different experts; among the rows of one device (aligned blocks of 128 tokens) no expert is named more than 32 times, a bound that some block reaches.
All inputs are finite; a program needn't handle non-finite values.
Results may differ from a plain program's by a relative error of at most 0.0071.
Values may be sent and summed in bfloat16 or wider, within the bound.
A program may use at most 128 MiB of HBM per device.

v0:
```python
import jax
import jax.numpy as jnp
from jax import lax
from jax.sharding import PartitionSpec as P


def with_halo(shard, sides, width):
    for axis, dim in sides:
        size, length = (lax.axis_size(axis), shard.shape[dim])
        up = [(i, (i + 1) % size) for i in range(size - 1)]
        down = [(j, i) for i, j in up]
        last = lax.slice_in_dim(shard, length - width, length, axis=dim)
        initial = lax.slice_in_dim(shard, 0, width, axis=dim)
        before = lax.ppermute(last, axis, up)
        after = lax.ppermute(initial, axis, down)
        shard = jnp.concatenate([before, shard, after], axis=dim)
    return shard


def expert_rows(rows, wg, wu, wd):
    gate = jnp.minimum(jnp.dot(rows, wg, preferred_element_type=jnp.float32), 7.0)
    upper = jnp.clip(jnp.dot(rows, wu, preferred_element_type=jnp.float32), -7.0, 7.0)
    act = ((upper + 1.0) * gate * jax.nn.sigmoid(1.702 * gate)).astype(jnp.bfloat16)
    return jnp.dot(act, wd, preferred_element_type=jnp.float32).astype(jnp.bfloat16)


def per_device(
    conv_in,
    gate_outer,
    gate_inner,
    tap_weights,
    doc_ids,
    w_proj,
    stream,
    norm_gain,
    routes,
    route_weights,
    w_gate,
    w_up,
    w_down,
):
    n_seq = lax.axis_size("sp")
    n_core = lax.axis_size("tp")
    tok_dev = conv_in.shape[0]
    width = w_proj.shape[1]
    topk = routes.shape[1]
    block = tok_dev // n_core
    n_expert = n_seq * n_core
    capacity = max(2, 2 * tok_dev * topk // (n_core * n_expert))
    product = gate_inner.astype(jnp.float32) * conv_in.astype(jnp.float32)
    doc_float = doc_ids.astype(jnp.float32)
    wide_prod, wide_docs = (
        with_halo(product, (("sp", 0),), 1),
        with_halo(doc_float, (("sp", 0),), 1),
    )
    same_before = (wide_docs[1:-1] == wide_docs[:-2]).astype(jnp.float32)
    same_after = (wide_docs[1:-1] == wide_docs[2:]).astype(jnp.float32)
    conv = (
        tap_weights[0] * wide_prod[:-2] * same_before[:, None]
        + tap_weights[1] * product
        + tap_weights[2] * wide_prod[2:] * same_after[:, None]
    )
    mixed = (gate_outer.astype(jnp.float32) * conv).astype(jnp.bfloat16)
    regrouped = lax.all_to_all(mixed, "tp", split_axis=0, concat_axis=1, tiled=True)
    projected = jnp.dot(regrouped, w_proj, preferred_element_type=jnp.float32)
    hidden = stream.astype(jnp.float32) + projected
    scale = lax.rsqrt(jnp.mean(hidden * hidden, axis=-1, keepdims=True) + 1e-05)
    normed = (hidden * scale * norm_gain).astype(jnp.bfloat16)
    chosen = routes.reshape(-1)
    onehot = (chosen[:, None] == jnp.arange(n_expert, dtype=jnp.int32)[None, :]).astype(jnp.int32)
    ranks = jnp.sum(jnp.cumsum(onehot, axis=0) * onehot, axis=-1) - 1
    places = chosen * capacity + ranks
    owners = jnp.arange(block * topk, dtype=jnp.int32) // topk
    outgoing = jnp.zeros((n_expert * capacity, width), jnp.bfloat16).at[places].set(normed[owners])
    arrived = lax.all_to_all(outgoing, ("sp", "tp"), split_axis=0, concat_axis=0, tiled=True)
    results = expert_rows(arrived, w_gate[0], w_up[0], w_down[0])
    returned = lax.all_to_all(results, ("sp", "tp"), split_axis=0, concat_axis=0, tiled=True)
    picked = returned[places].astype(jnp.float32) * route_weights.reshape(-1)[:, None]
    combined = jnp.sum(picked.reshape(block, topk, width), axis=1)
    return (hidden + combined).astype(jnp.bfloat16)


def solution(mesh):
    in_specs = (
        P("sp", "tp"),
        P("sp", "tp"),
        P("sp", "tp"),
        P(None, "tp"),
        P("sp"),
        P(),
        P(("sp", "tp"), None),
        P(),
        P(("sp", "tp"), None),
        P(("sp", "tp"), None),
        P(("sp", "tp"), None, None),
        P(("sp", "tp"), None, None),
        P(("sp", "tp"), None, None),
    )
    out_specs = P(("sp", "tp"), None)
    return jax.shard_map(
        per_device, mesh=mesh, in_specs=in_specs, out_specs=out_specs, check_vma=False
    )
```

profile of v0, /device:TPU:0, one launch (start us, length us, event | category | flops | bytes accessed | tf_op | source)
XLA Modules:
  0.0 285.6 jit_solution(8135735656092592648)
XLA Ops:
  1.4 5.4 %collective-permute-start.1 = (f32[1]{0:T(128)}, f32[1]{0:T(128)}, u32[]{:S(2)}, u32[]{:S(2)}) collective-permute-start(f32[1]{0:T(128)} %get-tuple-element.14), channel_id=1, source_target_pairs={{0,2},{2,4},{4,6},{6,8},{8,10},{10,12},{12,14},{14,16},{16,18},{18... | collective-permute-start | bytes 20 | tf_op jit(solution)/shard_map/ppermute | solution.py:14
  6.8 1.3 collective-permute-start.3
  8.1 1.1 convert_multiply_fusion
  10.0 4.5 %collective-permute-start = (f32[1,512]{1,0:T(1,128)S(1)}, f32[1,512]{1,0:T(1,128)S(1)}, u32[]{:S(2)}, u32[]{:S(2)}) collective-permute-start(f32[1,512]{1,0:T(1,128)S(1)} %get-tuple-element.5), channel_id=1, source_target_pairs={{0,2},{2,4},{4,6},{6,8},{8,10},{10,12},{12,14},{14,16},{16,18},{18... | collective-permute-start | bytes 6152 | tf_op jit(solution)/shard_map/ppermute | solution.py:14
  14.6 1.3 collective-permute-start.2
  18.4 1.2 reduce-window.6
  20.2 1.3 pad_maximum_fusion.2
  22.3 1.9 fusion.16
  24.2 4.7 %all_to_all.43 = bf16[2,128,512]{2,1,0:T(8,128)(2,1)} all-to-all(bf16[2,128,512]{2,1,0:T(8,128)(2,1)S(1)} %bitcast.51), channel_id=1, replica_groups=mesh['sp'=16,'tp'=2] {'tp'}, dimensions={0} | all-to-all | bytes 524288 | tf_op jit(solution)/shard_map/all_to_all | solution.py:64
  28.8 1.1 copy.20
  30.0 3.1 %multiply_reduce_fusion.1 = (f32[128]{0:T(128)S(1)}, f32[128,2048]{1,0:T(8,128)S(1)}) fusion(bf16[128,1024]{0,1:T(8,128)(2,1)S(1)} %bitcast.49, bf16[1024,2048]{1,0:T(8,128)(2,1)} %param.18, bf16[128,2048]{1,0:T(8,128)(2,1)} %param.19), kind=kOutput, calls=%fused_computation.17 | convolution fusion | flops 537919360 | bytes 6029824 | tf_op jit(solution)/shard_map/dot_general | solution.py:65
  33.1 1.0 copy-done.1
  34.1 0.9 multiply_convert_fusion.1
  35.0 12.4 %scatter_custom_fusion = bf16[1024,2048]{1,0:T(8,128)(2,1)} fusion(s32[512]{0:T(512)S(1)} %bitcast.55, bf16[128,2048]{1,0:T(8,128)(2,1)} %multiply_convert_fusion.1, s32[1024]{0:T(1024)S(1)} %pad_clamp_fusion.1, bf16[]{:T(256)} %constant.15.clone.1), kind=kCustom, calls=%fused_computation.12 | custom fusion | bytes 4194816 | tf_op jit(solution)/shard_map/scatter | solution.py:74
  47.4 101.8 %all_to_all.44 = bf16[32,32,2048]{2,1,0:T(8,128)(2,1)S(1)} all-to-all(bf16[32,32,2048]{2,1,0:T(8,128)(2,1)} %bitcast.45), channel_id=1, replica_groups=mesh['sp'=16,'tp'=2] {'sp','tp'}, dimensions={0} | all-to-all | bytes 8388608 | tf_op jit(solution)/shard_map/all_to_all | solution.py:75
  149.2 2.0 copy-done.3
  151.2 5.2 %fusion.1 = f32[1024,768]{1,0:T(8,128)} fusion(bf16[1024,2048]{1,0:T(8,128)(2,1)S(1)} %bitcast.47, bf16[1,2048,768]{2,1,0:T(8,128)(2,1)S(1)} %copy-done.7), kind=kOutput, calls=%fused_computation.6 | convolution fusion | flops 3221225472 | bytes 10485760 | tf_op jit(solution)/shard_map/dot_general | solution.py:21
  156.4 12.4 %convolution_convert_fusion = bf16[1024,2048]{1,0:T(8,128)(2,1)} fusion(bf16[1,768,2048]{2,1,0:T(8,128)(2,1)S(1)} %copy-done, f32[1024,768]{1,0:T(8,128)} %fusion.1, bf16[1024,2048]{1,0:T(8,128)(2,1)} %bitcast.48, bf16[1,2048,768]{2,1,0:T(8,128)(2,1)} %param.24), kind=kOutput, calls=%fused_computation.4 | convolution fusion | flops 6452412416 | bytes 17825792 | tf_op jit(solution)/shard_map/dot_general | solution.py:24
  168.8 4.0 %all-to-all-start.2 = ((bf16[32,32,2048]{2,1,0:T(8,128)(2,1)}), bf16[32,32,2048]{2,1,0:T(8,128)(2,1)}, u32[]{:S(2)}, u32[]{:S(2)}) async-start(bf16[32,32,2048]{2,1,0:T(8,128)(2,1)} %bitcast.46), calls=%async_computation.2 | async-start | bytes 8388608 | tf_op jit(solution)/shard_map/all_to_all | solution.py:77
  172.9 93.6 %all-to-all-done.2 = bf16[32,32,2048]{2,1,0:T(8,128)(2,1)} async-done(((bf16[32,32,2048]{2,1,0:T(8,128)(2,1)}), bf16[32,32,2048]{2,1,0:T(8,128)(2,1)}, u32[]{:S(2)}, u32[]{:S(2)}) %all-to-all-start.2) | async-done | bytes 4194336 | tf_op jit(solution)/shard_map/all_to_all | solution.py:77
  266.5 8.0 %gather_fusion = bf16[512,2048]{1,0:T(8,128)(2,1)} fusion(bf16[1024,2048]{1,0:T(8,128)(2,1)} %bitcast.16, s32[1024]{0:T(1024)S(1)} %pad_clamp_fusion), kind=kCustom, calls=%fused_computation.1 | custom fusion | bytes 4196352 | tf_op jit(solution)/shard_map/gather | solution.py:78
  274.4 4.7 %reshape.123 = f32[128,4,2048]{2,1,0:T(4,128)} reshape(bf16[512,2048]{1,0:T(8,128)(2,1)} %gather_fusion) | data formatting | bytes 6291456 | tf_op jit(solution)/shard_map/convert_element_type | solution.py:78
  279.2 5.5 %multiply_reduce_fusion = f32[128,2048]{1,0:T(8,128)S(1)} fusion(f32[128,4,2048]{2,1,0:T(4,128)} %reshape.123, f32[128,4]{1,0:T(8,128)S(1)} %copy.25), kind=kLoop, calls=%fused_computation.3 | loop fusion | flops 1835008 | bytes 5244928 | tf_op jit(solution)/shard_map/reduce_sum | solution.py:79
  284.7 0.9 add_convert_fusion
  (41 shorter events, 6.2 us)
Async XLA Ops:
  0.0 156.4 %copy-start = (bf16[1,768,2048]{2,1,0:T(8,128)(2,1)S(1)}, bf16[1,768,2048]{2,1,0:T(8,128)(2,1)}, u32[]{:S(2)}) copy-start(bf16[1,768,2048]{2,1,0:T(8,128)(2,1)} %param.25) | copy-start | bytes 9437188
  1.4 18.8 %collective-permute-start.1 = (f32[1]{0:T(128)}, f32[1]{0:T(128)}, u32[]{:S(2)}, u32[]{:S(2)}) collective-permute-start(f32[1]{0:T(128)} %get-tuple-element.14), channel_id=1, source_target_pairs={{0,2},{2,4},{4,6},{6,8},{8,10},{10,12},{12,14},{14,16},{16,18},{18... | collective-permute-start | bytes 20 | tf_op jit(solution)/shard_map/ppermute | solution.py:14
  6.8 13.4 %collective-permute-start.3 = (f32[1]{0:T(128)}, f32[1]{0:T(128)}, u32[]{:S(2)}, u32[]{:S(2)}) collective-permute-start(f32[1]{0:T(128)} %get-tuple-element.15), channel_id=1, source_target_pairs={{2,0},{4,2},{6,4},{8,6},{10,8},{12,10},{14,12},{16,14},{18,16},{20... | collective-permute-start | bytes 20 | tf_op jit(solution)/shard_map/ppermute | solution.py:15
  9.2 0.8 copy-start.4
  10.0 12.3 %collective-permute-start = (f32[1,512]{1,0:T(1,128)S(1)}, f32[1,512]{1,0:T(1,128)S(1)}, u32[]{:S(2)}, u32[]{:S(2)}) collective-permute-start(f32[1,512]{1,0:T(1,128)S(1)} %get-tuple-element.5), channel_id=1, source_target_pairs={{0,2},{2,4},{4,6},{6,8},{8,10},{10,12},{12,14},{14,16},{16,18},{18... | collective-permute-start | bytes 6152 | tf_op jit(solution)/shard_map/ppermute | solution.py:14
  14.6 7.7 %collective-permute-start.2 = (f32[1,512]{1,0:T(1,128)S(1)}, f32[1,512]{1,0:T(1,128)S(1)}, u32[]{:S(2)}, u32[]{:S(2)}) collective-permute-start(f32[1,512]{1,0:T(1,128)S(1)} %get-tuple-element.6), channel_id=1, source_target_pairs={{2,0},{4,2},{6,4},{8,6},{10,8},{12,10},{14,12},{16,14},{18,16},{20... | collective-permute-start | bytes 6152 | tf_op jit(solution)/shard_map/ppermute | solution.py:15
  30.0 4.1 %copy-start.5 = (f32[2048]{0:T(1024)S(1)}, f32[2048]{0:T(1024)}, u32[]{:S(2)}) copy-start(f32[2048]{0:T(1024)} %param.20) | copy-start | bytes 24580
  33.1 1.0 copy-start.1
  47.4 103.8 %copy-start.7 = (bf16[1,2048,768]{2,1,0:T(8,128)(2,1)S(1)}, bf16[1,2048,768]{2,1,0:T(8,128)(2,1)}, u32[]{:S(2)}) copy-start(bf16[1,2048,768]{2,1,0:T(8,128)(2,1)} %param.23) | copy-start | bytes 9437188
  149.2 2.0 copy-start.3
  168.8 4.0 %copy-start.6 = (f32[128,4]{0,1:T(4,128)S(1)}, f32[128,4]{0,1:T(4,128)}, u32[]{:S(2)}) copy-start(f32[128,4]{0,1:T(4,128)} %param.22) | copy-start | bytes 6148
  168.8 97.7 %all-to-all-start.2 = ((bf16[32,32,2048]{2,1,0:T(8,128)(2,1)}), bf16[32,32,2048]{2,1,0:T(8,128)(2,1)}, u32[]{:S(2)}, u32[]{:S(2)}) async-start(bf16[32,32,2048]{2,1,0:T(8,128)(2,1)} %bitcast.46), calls=%async_computation.2 | async-start | bytes 8388608 | tf_op jit(solution)/shard_map/all_to_all | solution.py:77
  279.2 5.5 %copy-start.2 = (f32[128,2048]{1,0:T(8,128)S(1)}, f32[128,2048]{1,0:T(8,128)}, u32[]{:S(2)}) copy-start(f32[128,2048]{1,0:T(8,128)} %copy-done.1) | copy-start | bytes 3145732
where the time goes:
time: 286 us
  blocking collectives  106 us (37%)
  waiting for transfers between devices  93.6 us (33%)
  local copies, waits for them, and re-layouts  32.9 us (12%)
  matrix products  20.7 us (7%)
  starting transfers between devices  16.6 us (6%)
  other arithmetic  15.2 us (5%)
    all_to_all x1, blocking collectives, per_device(): lax.all_to_all(outgoing, ('sp', 'tp'), split_axis=0, concat_axis=0, tiled...  102 us
    all_to_all x1, waiting for transfers between devices, per_device(): lax.all_to_all(results, ('sp', 'tp'), split_axis=0, concat_axis=0, tiled=...  93.6 us
    scatter x1, local copies, waits for them, and re-layouts, per_device(): jnp.zeros((n_expert * capacity, width), jnp.bfloat16).at[places]  12.4 us
    dot_general x1, matrix products, expert_rows(): jnp.dot(act, wd, preferred_element_type=jnp.float32).astype(jnp.bfloat16)  12.4 us
    ppermute x2, starting transfers between devices, with_halo(): before = lax.ppermute(last, axis, up)  9.97 us
    gather x1, local copies, waits for them, and re-layouts, per_device(): returned[places].astype(jnp.float32) * route_weights.reshape(-1)[:, None]  7.95 us
  transfers between devices with their start and end apart: 5, of which 1 were waited for; matrix products, arithmetic and copies ran while one was open for 3% of the time, Pallas kernels for 0%

commit v1 on v0

--- a/solution.py
+++ b/solution.py
@@ -1,7 +1,14 @@
+import functools
+import math
+
 import jax
 import jax.numpy as jnp
 from jax import lax
+from jax.experimental import pallas as pl
+from jax.experimental.pallas import tpu as pltpu
 from jax.sharding import PartitionSpec as P
+
+MESH = pl.DeviceIdType.MESH
 
 
 def with_halo(shard, sides, width):
@@ -17,11 +24,231 @@
     return shard
 
 
-def expert_rows(rows, wg, wu, wd):
-    gate = jnp.minimum(jnp.dot(rows, wg, preferred_element_type=jnp.float32), 7.0)
-    upper = jnp.clip(jnp.dot(rows, wu, preferred_element_type=jnp.float32), -7.0, 7.0)
-    act = ((upper + 1.0) * gate * jax.nn.sigmoid(1.702 * gate)).astype(jnp.bfloat16)
-    return jnp.dot(act, wd, preferred_element_type=jnp.float32).astype(jnp.bfloat16)
+def dot(a, b):
+    return jnp.dot(a, b, preferred_element_type=jnp.float32)
+
+
+def tile_of(size, most):
+    return next(t for t in range(most, 0, -128) if size % t == 0)
+
+
+def schedule(steps):
+    order, d, f, c = [], 0, 0, 0
+    while c < steps:
+        while d < steps and d < f + 2:
+            order.append(("d", d))
+            d += 1
+        if f < steps:
+            order.append(("f", f))
+            f += 1
+        if f - c >= 2 or f == steps:
+            order.append(("c", c))
+            c += 1
+    return order
+
+
+def moe_kernel(
+    nz, n_plane, n_core, cap,
+    normed, hidden, select, spread, wg_hbm, wu_hbm, wd_hbm,
+    out_ref,
+    wg, wu, wd, zbuf, outgoing, arrived, act, results, returned, partial, summed,
+    w_sem, z_send, z_recv, a_send, a_recv, r_send, r_recv, p_send, p_recv,
+):
+    peers = n_plane * n_core
+    width = normed.shape[1]
+    rows = peers * cap
+    ff = wg.shape[1]
+    me = lax.axis_index("sp")
+    core = lax.axis_index("tp")
+    z, p = me // n_plane, lax.rem(me, n_plane)
+    rank = p * n_core + core
+
+    def z_peer(k):
+        return {"sp": lax.rem(z + k, nz) * n_plane + p, "tp": core}
+
+    def plane_peer(j):
+        q = lax.rem(rank + j, peers)
+        return {"sp": z * n_plane + q // n_core, "tp": lax.rem(q, n_core)}
+
+    loads = [
+        pltpu.make_async_copy(src, dst, w_sem.at[i])
+        for i, (src, dst) in enumerate(((wg_hbm, wg), (wu_hbm, wu), (wd_hbm, wd)))
+    ]
+    for load in loads:
+        load.start()
+    barrier = pltpu.get_barrier_semaphore()
+    for k in range(1, nz):
+        pl.semaphore_signal(barrier, inc=1, device_id=z_peer(k), device_id_type=MESH)
+    for j in range(1, peers):
+        pl.semaphore_signal(barrier, inc=1, device_id=plane_peer(j), device_id_type=MESH)
+    pl.semaphore_wait(barrier, nz - 1 + peers - 1)
+
+    def remote(src, dst, send, recv, to):
+        return pltpu.make_async_remote_copy(
+            src_ref=src, dst_ref=dst, send_sem=send, recv_sem=recv,
+            device_id=to, device_id_type=MESH)
+
+    z_copies = {}
+    for k in range(1, nz):
+        z_copies[k] = remote(normed, zbuf.at[k - 1], z_send.at[k], z_recv.at[k], z_peer(k))
+        z_copies[k].start()
+
+    a_copies, r_copies, p_copies = {}, {}, {}
+    col = tile_of(width, 512)
+    fcol = tile_of(ff, 256)
+
+    def dispatch(k):
+        if k:
+            z_copies[k].wait_recv()
+        block = normed if k == 0 else zbuf.at[k - 1]
+
+        @pl.loop(0, width // col)
+        def _(i):
+            cols = pl.ds(pl.multiple_of(i * col, col), col)
+            picked = dot(select[k], block[:, cols]).astype(jnp.bfloat16)
+            arrived[k, 0:cap, cols] = picked[:cap]
+            outgoing[k, :, cols] = picked[cap:]
+
+        for j in range(1, peers):
+            a_copies[k, j] = remote(
+                outgoing.at[k, pl.ds((j - 1) * cap, cap)], arrived.at[k, pl.ds(j * cap, cap)],
+                a_send.at[k, j], a_recv.at[k, j], plane_peer(j))
+            a_copies[k, j].start()
+
+    def expert(k):
+        if k == 0:
+            for load in loads:
+                load.wait()
+        for j in range(1, peers):
+            a_copies[k, j].wait_recv()
+
+        @pl.loop(0, ff // fcol)
+        def _(i):
+            cols = pl.ds(pl.multiple_of(i * fcol, fcol), fcol)
+            gate = jnp.minimum(dot(arrived[k], wg[:, cols]), 7.0)
+            upper = jnp.clip(dot(arrived[k], wu[:, cols]), -7.0, 7.0)
+            act[:, cols] = ((upper + 1.0) * gate * jax.nn.sigmoid(1.702 * gate)).astype(jnp.bfloat16)
+
+        @pl.loop(0, width // col)
+        def _(i):
+            cols = pl.ds(pl.multiple_of(i * col, col), col)
+            res = dot(act[...], wd[:, cols]).astype(jnp.bfloat16)
+            returned[k, 0:cap, cols] = res[:cap]
+            results[k, :, cols] = res[cap:]
+
+        for j in range(1, peers):
+            r_copies[k, j] = remote(
+                results.at[k, pl.ds((j - 1) * cap, cap)], returned.at[k, pl.ds(j * cap, cap)],
+                r_send.at[k, j], r_recv.at[k, j], plane_peer(peers - j))
+            r_copies[k, j].start()
+
+    def combine(k):
+        for j in range(1, peers):
+            r_copies[k, j].wait_recv()
+
+        @pl.loop(0, width // col)
+        def _(i):
+            cols = pl.ds(pl.multiple_of(i * col, col), col)
+            total = dot(spread[k], returned[k, :, cols])
+            if k == 0:
+                hidden[:, cols] = hidden[:, cols] + total
+            else:
+                partial[k - 1, :, cols] = total.astype(jnp.bfloat16)
+
+        if k:
+            p_copies[k] = remote(
+                partial.at[k - 1], summed.at[k - 1], p_send.at[k], p_recv.at[k], z_peer(nz - k))
+            p_copies[k].start()
+
+    for kind, k in schedule(nz):
+        {"d": dispatch, "f": expert, "c": combine}[kind](k)
+
+    for k in range(1, nz):
+        p_copies[k].wait_recv()
+
+    @pl.loop(0, width // col)
+    def _(i):
+        cols = pl.ds(pl.multiple_of(i * col, col), col)
+        total = hidden[:, cols]
+        for k in range(1, nz):
+            total = total + summed[k - 1, :, cols].astype(jnp.float32)
+        out_ref[:, cols] = total.astype(jnp.bfloat16)
+
+    for k in range(1, nz):
+        z_copies[k].wait_send()
+        p_copies[k].wait_send()
+    for k in range(nz):
+        for j in range(1, peers):
+            a_copies[k, j].wait_send()
+            r_copies[k, j].wait_send()
+
+
+def moe(nz, n_plane, n_core, cap, normed, hidden, select, spread, wg, wu, wd):
+    block, width = normed.shape
+    ff = wg.shape[1]
+    peers = n_plane * n_core
+    rows = peers * cap
+    bf = jnp.bfloat16
+    vmem = pl.BlockSpec(memory_space=pltpu.VMEM)
+    hbm = pl.BlockSpec(memory_space=pl.ANY)
+    dma = pltpu.SemaphoreType.DMA
+
+    def body(normed, hidden_in, *rest):
+        hidden = rest[-1]
+        hidden[...] = hidden_in[...]
+        moe_kernel(nz, n_plane, n_core, cap, normed, hidden, *rest[:-1])
+
+    return pl.pallas_call(
+        body,
+        out_shape=jax.ShapeDtypeStruct((block, width), bf),
+        in_specs=[vmem] * 4 + [hbm] * 3,
+        out_specs=vmem,
+        scratch_shapes=[
+            pltpu.VMEM((width, ff), bf),
+            pltpu.VMEM((width, ff), bf),
+            pltpu.VMEM((ff, width), bf),
+            pltpu.VMEM((nz - 1, block, width), bf),
+            pltpu.VMEM((nz, rows - cap, width), bf),
+            pltpu.VMEM((nz, rows, width), bf),
+            pltpu.VMEM((rows, ff), bf),
+            pltpu.VMEM((nz, rows - cap, width), bf),
+            pltpu.VMEM((nz, rows, width), bf),
+            pltpu.VMEM((nz - 1, block, width), bf),
+            pltpu.VMEM((nz - 1, block, width), bf),
+            dma((3,)), dma((nz,)), dma((nz,)),
+            dma((nz, peers)), dma((nz, peers)), dma((nz, peers)), dma((nz, peers)),
+            dma((nz,)), dma((nz,)),
+            pltpu.VMEM((block, width), jnp.float32),
+        ],
+        compiler_params=pltpu.CompilerParams(
+            collective_id=0, has_side_effects=True, vmem_limit_bytes=60 * 2**20),
+        name="moe_exchange",
+    )(normed, hidden, select, spread, wg, wu, wd)
+
+
+def slot_matrices(nz, n_plane, n_core, cap, routes, route_weights):
+    block, topk = routes.shape
+    peers = n_plane * n_core
+    me = lax.axis_index("sp")
+    z, p = me // n_plane, lax.rem(me, n_plane)
+    rank = p * n_core + lax.axis_index("tp")
+    groups = [[a * n_plane + b for a in range(nz)] for b in range(n_plane)]
+    packed = jnp.concatenate([routes.astype(jnp.float32), route_weights], axis=1)
+    every = lax.all_gather(packed, "sp", axis_index_groups=groups)
+    every = every[(z - jnp.arange(nz)) % nz]
+    chosen, weight = every[..., :topk].astype(jnp.int32), every[..., topk:]
+    experts = z * peers + (rank + jnp.arange(peers)) % peers
+    hit = chosen[..., None] == experts
+    named = jnp.any(hit, axis=2)
+    share = jnp.sum(jnp.where(hit, weight[..., None], 0.0), axis=2)
+    below = jnp.tril(jnp.ones((block, block), jnp.bfloat16), -1)
+    slot = jnp.einsum("ts,kse->kte", below, named.astype(jnp.bfloat16), preferred_element_type=jnp.float32)
+    slot = jnp.where(named, slot.astype(jnp.int32), -1)
+    place = slot[..., None] == jnp.arange(cap, dtype=jnp.int32)
+    spread = jnp.where(place, share[..., None], 0.0).astype(jnp.bfloat16).reshape(nz, block, peers * cap)
+    slot_t = jnp.swapaxes(slot, 1, 2)
+    select = (slot_t[:, :, None, :] == jnp.arange(cap, dtype=jnp.int32)[:, None]).astype(jnp.bfloat16)
+    return select.reshape(nz, peers * cap, block), spread
 
 
 def per_device(
@@ -42,11 +269,13 @@
     n_seq = lax.axis_size("sp")
     n_core = lax.axis_size("tp")
     tok_dev = conv_in.shape[0]
-    width = w_proj.shape[1]
     topk = routes.shape[1]
-    block = tok_dev // n_core
     n_expert = n_seq * n_core
     capacity = max(2, 2 * tok_dev * topk // (n_core * n_expert))
+    capacity = -(-capacity // 16) * 16
+    nz = max(d for d in range(1, math.isqrt(n_seq) + 1) if n_seq % d == 0)
+    n_plane = n_seq // nz
+    select, spread = slot_matrices(nz, n_plane, n_core, capacity, routes, route_weights)
     product = gate_inner.astype(jnp.float32) * conv_in.astype(jnp.float32)
     doc_float = doc_ids.astype(jnp.float32)
     wide_prod, wide_docs = (
@@ -66,18 +295,7 @@
     hidden = stream.astype(jnp.float32) + projected
     scale = lax.rsqrt(jnp.mean(hidden * hidden, axis=-1, keepdims=True) + 1e-05)
     normed = (hidden * scale * norm_gain).astype(jnp.bfloat16)
-    chosen = routes.reshape(-1)
-    onehot = (chosen[:, None] == jnp.arange(n_expert, dtype=jnp.int32)[None, :]).astype(jnp.int32)
-    ranks = jnp.sum(jnp.cumsum(onehot, axis=0) * onehot, axis=-1) - 1
-    places = chosen * capacity + ranks
-    owners = jnp.arange(block * topk, dtype=jnp.int32) // topk
-    outgoing = jnp.zeros((n_expert * capacity, width), jnp.bfloat16).at[places].set(normed[owners])
-    arrived = lax.all_to_all(outgoing, ("sp", "tp"), split_axis=0, concat_axis=0, tiled=True)
-    results = expert_rows(arrived, w_gate[0], w_up[0], w_down[0])
-    returned = lax.all_to_all(results, ("sp", "tp"), split_axis=0, concat_axis=0, tiled=True)
-    picked = returned[places].astype(jnp.float32) * route_weights.reshape(-1)[:, None]
-    combined = jnp.sum(picked.reshape(block, topk, width), axis=1)
-    return (hidden + combined).astype(jnp.bfloat16)
+    return moe(nz, n_plane, n_core, capacity, normed, hidden, select, spread, w_gate[0], w_up[0], w_down[0])
 
 
 def solution(mesh):

time: 286 us -> 183 us (0.64)
  Pallas kernels: 0 us -> 132 us
  waiting for transfers between devices: 93.6 us -> 0.01 us
  blocking collectives: 106 us -> 21.6 us
  local copies, waits for them, and re-layouts: 32.9 us -> 4.54 us
  matrix products: 20.7 us -> 3.21 us
  other arithmetic: 15.2 us -> 7.82 us
  starting transfers between devices: 16.6 us -> 12.5 us
    pallas_call x0 -> x1, Pallas kernels: none -> 132 us  [moe(): pl.pallas_call(body, out_shape=jax.ShapeDtypeStruct((block, width), bf),...]
    all_to_all x1 -> x0, blocking collectives: 102 us -> none  [per_device(): lax.all_to_all(outgoing, ('sp', 'tp'), split_axis=0, concat_axis=0, tiled...]
    all_to_all x1 -> x0, waiting for transfers between devices: 93.6 us -> none  [per_device(): lax.all_to_all(results, ('sp', 'tp'), split_axis=0, concat_axis=0, tiled=...]
    all_gather x0 -> x1, blocking collectives: none -> 17.6 us  [slot_matrices(): every = lax.all_gather(packed, 'sp', axis_index_groups=groups)]
    dot_general x2 -> x1, matrix products: 17.6 us -> 0.2 us  [slot_matrices(): jnp.einsum('ts,kse->kte', below, named.astype(jnp.bfloat16), preferred_el...]
    scatter x1 -> x0, local copies, waits for them, and re-layouts: 12.4 us -> none  [per_device(): jnp.zeros((n_expert * capacity, width), jnp.bfloat16).at[places]]
    gather x1, local copies, waits for them, and re-layouts: 7.95 us -> 0.55 us  [slot_matrices(): every = every[(z - jnp.arange(nz)) % nz]]
    reduce_sum x2 -> x1, other arithmetic: 5.61 us -> 0.08 us  [slot_matrices(): share = jnp.sum(jnp.where(hit, weight[..., None], 0.0), axis=2)]
  transfers between devices with their start and end apart: 5 -> 4, of which waited for: 1 -> 0; matrix products, arithmetic and copies ran while one was open for 3% -> 4% of each run, Pallas kernels for 0% -> 0%
where the time goes in v1:
time: 183 us; the launch traced here: 182 us
  Pallas kernels  132 us (72%)
  blocking collectives  21.6 us (12%)
  starting transfers between devices  12.5 us (7%)
  other arithmetic  7.82 us (4%)
  local copies, waits for them, and re-layouts  4.54 us (2%)
  matrix products  3.21 us (2%)
    pallas_call x1, Pallas kernels, moe(): pl.pallas_call(body, out_shape=jax.ShapeDtypeStruct((block, width), bf),...  132 us
    all_gather x1, blocking collectives, slot_matrices(): every = lax.all_gather(packed, 'sp', axis_index_groups=groups)  17.6 us
    ppermute x2, starting transfers between devices, with_halo(): before = lax.ppermute(last, axis, up)  9.97 us
    all_to_all x1, blocking collectives, per_device(): lax.all_to_all(mixed, 'tp', split_axis=0, concat_axis=1, tiled=True)  3.94 us
  transfers between devices with their start and end apart: 4, of which 0 were waited for; matrix products, arithmetic and copies ran while one was open for 4% of the time, Pallas kernels for 0%

profile of v1, /device:TPU:0, one launch (start us, length us, event | category | flops | bytes accessed | tf_op | source)
XLA Modules:
  0.0 182.4 jit_solution(10464259832589240239)
XLA Ops:
  0.0 0.8 convert_element_type.53
  0.8 0.6 fusion.25
  1.3 5.4 %collective-permute-start.1 = (f32[1]{0:T(128)}, f32[1]{0:T(128)}, u32[]{:S(2)}, u32[]{:S(2)}) collective-permute-start(f32[1]{0:T(128)} %get-tuple-element.16), channel_id=1, source_target_pairs={{0,2},{2,4},{4,6},{6,8},{8,10},{10,12},{12,14},{14,16},{16,18},{18... | collective-permute-start | bytes 20 | tf_op jit(solution)/shard_map/ppermute | solution.py:21
  6.8 1.3 collective-permute-start.3
  8.1 1.1 convert_multiply_fusion
  9.2 4.5 %collective-permute-start = (f32[1,512]{1,0:T(1,128)S(1)}, f32[1,512]{1,0:T(1,128)S(1)}, u32[]{:S(2)}, u32[]{:S(2)}) collective-permute-start(f32[1,512]{1,0:T(1,128)S(1)} %get-tuple-element.5), channel_id=1, source_target_pairs={{0,2},{2,4},{4,6},{6,8},{8,10},{10,12},{12,14},{14,16},{16,18},{18... | collective-permute-start | bytes 6152 | tf_op jit(solution)/shard_map/ppermute | solution.py:21
  13.7 1.3 collective-permute-start.2
  15.1 0.7 convert_element_type.58
  15.9 0.8 fusion.24
  16.7 0.7 pad_maximum_fusion.2
  17.4 17.6 %all-gather = f32[512,8]{0,1:T(8,128)S(1)} all-gather(f32[128,8]{0,1:T(8,128)S(1)} %pad_maximum_fusion.2), channel_id=2, replica_groups={{0,8,16,24},{2,10,18,26},{4,12,20,28},{6,14,22,30},{1,9,17,25},{3,11,19..., dimensions={0}, use_global_device_ids=true | all-gather | bytes 20480 | tf_op jit(solution)/shard_map/all_gather | solution.py:237
  35.0 0.5 gather_fusion
  35.8 0.2 bitcast_select_fusion.1
  36.2 0.2 copy.27
  36.4 0.8 fusion.8.rest_0_
  37.3 0.8 select_convert_fusion.rest_1_
  38.0 1.3 pad_maximum_fusion.3
  39.5 0.3 fusion.4
  39.7 3.9 %all_to_all.19 = bf16[2,128,512]{2,1,0:T(8,128)(2,1)S(1)} all-to-all(bf16[2,128,512]{2,1,0:T(8,128)(2,1)S(1)} %bitcast.38), channel_id=1, replica_groups=mesh['sp'=16,'tp'=2] {'tp'}, dimensions={0} | all-to-all | bytes 524288 | tf_op jit(solution)/shard_map/all_to_all | solution.py:293
  43.7 0.2 copy.26
  43.9 3.0 %multiply_reduce_fusion = (f32[128]{0:T(128)S(1)}, f32[128,2048]{1,0:T(8,128)S(1)}) fusion(bf16[128,1024]{0,1:T(8,128)(2,1)S(1)} %bitcast.35, bf16[1024,2048]{1,0:T(8,128)(2,1)} %param.18, bf16[128,2048]{1,0:T(8,128)(2,1)S(1)} %copy-done.1), kind=kOutput, calls=%fused_computation.4 | convolution fusion | flops 537919360 | bytes 6029824 | tf_op jit(solution)/shard_map/dot_general | solution.py:294
  46.9 1.1 multiply_convert_fusion.normed
  48.0 132.5 %moe_exchange.1 = bf16[128,2048]{1,0:T(8,128)(2,1)} custom-call(bf16[128,2048]{1,0:T(8,128)(2,1)} %multiply_convert_fusion.normed, f32[128,2048]{1,0:T(8,128)} %copy-done, bf16[4,256,128]{2,1,0:T(8,128)(2,1)} %fusion.8.rest_0_, bf16[4,128,256]{2,1,0:T(8,128)(2,1)} %select_convert_fusion.rest_1_, bf16[2048,768]{1,0:T(8,128)(2,1)} %bitcast.31, ...), custom_call_target="tpu_custom_call" | custom-call | tf_op jit(solution)/shard_map/moe_exchange/pallas_call | solution.py:201
  180.5 1.9 %copy.30 = bf16[128,2048]{1,0:T(8,128)(2,1)} copy(bf16[128,2048]{1,0:T(8,128)(2,1)} %moe_exchange.1) | data formatting | bytes 1048576
  (30 shorter events, 0.6 us)
Async XLA Ops:
  0.0 39.4 %copy-start.4 = (s32[256]{0:T(256)S(1)}, s32[256]{0:T(256)}, u32[]{:S(2)}) copy-start(s32[256]{0:T(256)} %param.17) | copy-start | bytes 3076
  0.0 39.5 %copy-start.2 = (bf16[256,512]{1,0:T(8,128)(2,1)S(1)}, bf16[256,512]{1,0:T(8,128)(2,1)}, u32[]{:S(2)}) copy-start(bf16[256,512]{1,0:T(8,128)(2,1)} %param.14) | copy-start | bytes 786436
  0.0 43.9 %copy-start.1 = (bf16[128,2048]{1,0:T(8,128)(2,1)S(1)}, bf16[128,2048]{1,0:T(8,128)(2,1)}, u32[]{:S(2)}) copy-start(bf16[128,2048]{1,0:T(8,128)(2,1)} %param.19) | copy-start | bytes 1572868
  1.3 36.7 %collective-permute-start.1 = (f32[1]{0:T(128)}, f32[1]{0:T(128)}, u32[]{:S(2)}, u32[]{:S(2)}) collective-permute-start(f32[1]{0:T(128)} %get-tuple-element.16), channel_id=1, source_target_pairs={{0,2},{2,4},{4,6},{6,8},{8,10},{10,12},{12,14},{14,16},{16,18},{18... | collective-permute-start | bytes 20 | tf_op jit(solution)/shard_map/ppermute | solution.py:21
  6.8 31.3 %collective-permute-start.3 = (f32[1]{0:T(128)}, f32[1]{0:T(128)}, u32[]{:S(2)}, u32[]{:S(2)}) collective-permute-start(f32[1]{0:T(128)} %get-tuple-element.17), channel_id=1, source_target_pairs={{2,0},{4,2},{6,4},{8,6},{10,8},{12,10},{14,12},{16,14},{18,16},{20... | collective-permute-start | bytes 20 | tf_op jit(solution)/shard_map/ppermute | solution.py:22
  9.2 30.3 %collective-permute-start = (f32[1,512]{1,0:T(1,128)S(1)}, f32[1,512]{1,0:T(1,128)S(1)}, u32[]{:S(2)}, u32[]{:S(2)}) collective-permute-start(f32[1,512]{1,0:T(1,128)S(1)} %get-tuple-element.5), channel_id=1, source_target_pairs={{0,2},{2,4},{4,6},{6,8},{8,10},{10,12},{12,14},{14,16},{16,18},{18... | collective-permute-start | bytes 6152 | tf_op jit(solution)/shard_map/ppermute | solution.py:21
  13.7 25.7 %collective-permute-start.2 = (f32[1,512]{1,0:T(1,128)S(1)}, f32[1,512]{1,0:T(1,128)S(1)}, u32[]{:S(2)}, u32[]{:S(2)}) collective-permute-start(f32[1,512]{1,0:T(1,128)S(1)} %get-tuple-element.6), channel_id=1, source_target_pairs={{2,0},{4,2},{6,4},{8,6},{10,8},{12,10},{14,12},{16,14},{18,16},{20... | collective-permute-start | bytes 6152 | tf_op jit(solution)/shard_map/ppermute | solution.py:22
  38.0 8.9 %copy-start.3 = (f32[2048]{0:T(1024)S(1)}, f32[2048]{0:T(1024)}, u32[]{:S(2)}) copy-start(f32[2048]{0:T(1024)} %param.20) | copy-start | bytes 24580
  46.9 1.2 copy-start
